TPU v7x, 128 devices: a whole 4x4x4 slice. The times are simulated.
128 devices in a mesh: sp: 64 (over z, y, x), tp: 2 (over core).
Axes of the slice: x: 4, y: 4, z: 4, core: 2. Of those that a mesh axis runs over, the one named last changes fastest.
Arguments:
- residual: bfloat16 [16384, 2048], P(('sp', 'tp')), may hold values from -6 to 6
- queries: bfloat16 [16384, 1024], P('sp', 'tp'), may hold values from -6 to 6
- keys: bfloat16 [16384, 1024], P('sp', 'tp'), may hold values from -6 to 6
- values: bfloat16 [16384, 2048], P('sp', 'tp'), may hold values from -6 to 6
- out_gate: bfloat16 [16384, 2048], P('sp', 'tp'), may hold values from -6 to 6
- in_gate: float32 [2, 16384, 8], P(None, 'sp', 'tp'), may hold values from -6 to 140, as said below
- forget_gate: float32 [2, 16384, 8], P(None, 'sp', 'tp'), may hold values from 0 to 20
- head_gain: float32 [2048], P('tp'), may hold values from 0.1 to 1.9
- w_out: bfloat16 [2048, 2048], P('tp'), may hold values from -0.125 to 0.125
- norm_gain: float32 [2048], replicated, may hold values from 0.1 to 1.9
- shared_gate: bfloat16 [2048, 512], replicated, may hold values from -0.125 to 0.125
- shared_up: bfloat16 [2048, 512], replicated, may hold values from -0.125 to 0.125
- shared_down: bfloat16 [512, 2048], replicated, may hold values from -0.25 to 0.25
- w_gate: bfloat16 [128, 2048, 512], P(('sp', 'tp')), may hold values from -0.125 to 0.125
- w_up: bfloat16 [128, 2048, 512], P(('sp', 'tp')), may hold values from -0.125 to 0.125
- w_down: bfloat16 [128, 512, 2048], P(('sp', 'tp')), may hold values from -0.25 to 0.25
- routes: int32 [16384, 4], P(('sp', 'tp')), may hold values from 0 to 127, all different within a row; in each aligned block of 128 rows (0 to 127, 128 to 255, ...) at most 8 rows name the same one
- route_weight: float32 [16384, 4], P(('sp', 'tp')), may hold values from 0.3 to 1.5
Outputs:
- layer_out: bfloat16 [16384, 2048], P(('sp', 'tp'))
Inputs may be any that keep to these rules, and one draw needn't show every extreme that they name: `in_gate`: log input gates mostly of order one. `routes`: each row names 4 different experts. Among the rows of one device (aligned blocks of 128 rows) no expert is named more than 8 times, a bound that some block reaches.
All inputs are finite; a program needn't handle non-finite values.
Results may differ from a plain program's by a relative error of at most 0.017.
Values may be sent and summed in bfloat16 or wider, within the bound.
A program may use at most 128 MiB of HBM per device.

v0:
```python
import math

import jax
import jax.numpy as jnp
from jax import lax
from jax.sharding import Mesh
from jax.sharding import PartitionSpec as P

SP = ("sp_0", "sp_1", "sp_2")
SP_TP = ("sp_0", "sp_1", "sp_2", "tp")


epsilon = 1e-06
max_floor = -1e30


def nothing_yet(value, identity):
    return jax.tree.map(
        lambda part, zero: jnp.zeros_like(part) + jnp.asarray(zero, part.dtype), value, identity
    )


def prefix_by_axis(value, axes, combine, identity):
    before = start = nothing_yet(value, identity)
    total = value
    for axis in reversed(axes):
        count, here = (lax.axis_size(axis), lax.axis_index(axis))
        pieces = jax.tree.map(lambda part: lax.all_gather(part, axis), total)
        inside, total = (start, start)
        for k in reversed(range(count)):
            passed = k > here
            total = combine(total, jax.tree.map(lambda part: part[k], pieces))
            inside = jax.tree.map(lambda new, old: jnp.where(passed, new, old), total, inside)
        before = combine(inside, before)
    return before


def gathered_once(value, axis):
    leaves = jax.tree.leaves(value)
    sequence = sorted(range(len(leaves)), key=lambda k: -leaves[k].size)
    width = (1, *leaves[sequence[0]].shape)[-1]
    lines = [
        jnp.pad(leaves[k].reshape(-1), (0, -leaves[k].size % width)).reshape(-1, width)
        for k in sequence
    ]
    both, at, found = (lax.all_gather(jnp.concatenate(lines), axis), 0, {})
    for k, line in zip(sequence, lines):
        slab = both[:, at : at + len(line)].reshape(len(both), -1)
        found[k] = slab[:, : leaves[k].size].reshape(-1, *leaves[k].shape)
        at += len(line)
    numbers = iter(range(len(leaves)))
    return jax.tree.map(lambda _: found[next(numbers)], value)


def entering(value, axes, combine, identity):
    before = start = nothing_yet(value, identity)
    total = value
    for axis in reversed(axes):
        count, here = (lax.axis_size(axis), lax.axis_index(axis))
        pieces = gathered_once(total, axis)
        inside, total = (start, start)
        for k in range(count):
            passed = k < here
            total = combine(total, jax.tree.map(lambda part: part[k], pieces))
            inside = jax.tree.map(lambda new, old: jnp.where(passed, new, old), total, inside)
        before = combine(inside, before)
    return before


def in_blocks(value, dim, count):
    before, after = (value.shape[:dim], value.shape[dim + 1 :])
    return jnp.moveaxis(value.reshape(*before, count, -1, *after), dim, 0)


def sum_at_owner(value, axis, dim):
    count = lax.axis_size(axis)
    blocks = lax.all_to_all(in_blocks(value, dim, count), axis, 0, 0, tiled=True)
    return jnp.sum(blocks.astype(jnp.float32), axis=0)


def combine_states(earlier, later):
    early_matrix, early_norm, early_max, early_decay = earlier
    late_matrix, late_norm, late_max, late_decay = later
    joined_max = jnp.maximum(late_decay + early_max, late_max)
    early_scale = jnp.exp(late_decay + early_max - joined_max)
    late_scale = jnp.exp(late_max - joined_max)
    joined_matrix = (
        early_scale[:, None, None] * early_matrix + late_scale[:, None, None] * late_matrix
    )
    joined_norm = early_scale[:, None] * early_norm + late_scale[:, None] * late_norm
    return (joined_matrix, joined_norm, joined_max, early_decay + late_decay)


def cell_direction(query_heads, key_heads, value_heads, gate_input, log_forget, backward):
    if backward:
        query_heads = query_heads[::-1]
        key_heads = key_heads[::-1]
        value_heads = value_heads[::-1]
        gate_input = gate_input[::-1]
        log_forget = log_forget[::-1]
    row_count, head_count, key_dim = key_heads.shape
    key_scale = 1.0 / math.sqrt(key_dim)
    running = jnp.cumsum(log_forget, axis=0)
    block_decay = running[-1]
    log_weight = block_decay[None, :] - running + gate_input
    block_max = jnp.max(log_weight, axis=0)
    scaled = jnp.exp(log_weight - block_max[None, :]) * key_scale
    weighted_keys = lax.optimization_barrier((key_heads * scaled[:, :, None]).astype(jnp.bfloat16))
    block_matrix = jnp.einsum(
        "thd,the->hde", weighted_keys, value_heads, preferred_element_type=jnp.float32
    )
    block_norm = jnp.sum(weighted_keys.astype(jnp.float32), axis=0)
    summary = (block_matrix, block_norm, block_max, block_decay)
    identity = (
        jnp.zeros_like(block_matrix),
        jnp.zeros_like(block_norm),
        jnp.full_like(block_max, max_floor),
        jnp.zeros_like(block_decay),
    )
    if backward:
        carried = prefix_by_axis(summary, SP, combine_states, identity)
    else:
        carried = entering(summary, SP, combine_states, identity)
    state_matrix, state_norm, state_max, unused_decay = carried
    lower = jnp.tril(jnp.ones((row_count, row_count), dtype=bool))
    running_heads = running.T
    pair_log = running_heads[:, :, None] - running_heads[:, None, :] + gate_input.T[:, None, :]
    pair_log = jnp.where(lower[None], pair_log, -jnp.inf)
    crossing_peak = running_heads + state_max[:, None]
    row_max = jnp.maximum(crossing_peak, jnp.max(pair_log, axis=2))
    scores = (
        jnp.einsum("thd,shd->hts", query_heads, key_heads, preferred_element_type=jnp.float32)
        * key_scale
    )
    cell_weight = jnp.exp(pair_log - row_max[:, :, None]) * scores
    weight_low = cell_weight.astype(jnp.bfloat16)
    inter_scale = jnp.exp(crossing_peak - row_max)
    query_wide = query_heads.astype(jnp.float32)
    read_state = jnp.einsum(
        "thd,hde->hte", query_wide, state_matrix, precision=lax.Precision.HIGHEST
    )
    read_norm = jnp.einsum("thd,hd->ht", query_wide, state_norm, precision=lax.Precision.HIGHEST)
    local_part = jnp.einsum(
        "hts,she->hte", weight_low, value_heads, preferred_element_type=jnp.float32
    )
    numerator = inter_scale[:, :, None] * read_state + local_part
    denominator = inter_scale * read_norm + jnp.sum(cell_weight, axis=2)
    result = numerator / jnp.maximum(jnp.abs(denominator), jnp.exp(-row_max))[:, :, None]
    result = jnp.transpose(result, (1, 0, 2))
    if backward:
        result = result[::-1]
    return result


def local(
    residual,
    queries,
    keys,
    values,
    out_gate,
    in_gate,
    forget_gate,
    head_gain,
    w_out,
    norm_gain,
    shared_gate,
    shared_up,
    shared_down,
    w_gate,
    w_up,
    w_down,
    routes,
    route_weight,
):
    row_count = queries.shape[0]
    local_heads = in_gate.shape[2]
    key_dim = queries.shape[1] // local_heads
    value_dim = values.shape[1] // local_heads
    query_heads = queries.reshape(row_count, local_heads, key_dim)
    key_heads = keys.reshape(row_count, local_heads, key_dim)
    value_heads = values.reshape(row_count, local_heads, value_dim)
    log_forget = jax.nn.log_sigmoid(forget_gate)
    forward_out = cell_direction(
        query_heads, key_heads, value_heads, in_gate[0], log_forget[0], False
    )
    backward_out = cell_direction(
        query_heads, key_heads, value_heads, in_gate[1], log_forget[1], True
    )
    summed = forward_out + backward_out
    normal = summed * lax.rsqrt(jnp.mean(summed * summed, axis=-1, keepdims=True) + epsilon)
    mixed_heads = (
        normal.reshape(row_count, local_heads * value_dim)
        * head_gain
        * jax.nn.sigmoid(out_gate.astype(jnp.float32))
    ).astype(jnp.bfloat16)
    own_rows = residual.shape[0]
    model_width = residual.shape[1]
    projected = sum_at_owner(
        jnp.dot(mixed_heads, w_out, preferred_element_type=jnp.float32).astype(jnp.bfloat16),
        "tp",
        0,
    )
    updated = (residual.astype(jnp.float32) + projected).astype(jnp.bfloat16)
    updated_wide = updated.astype(jnp.float32)
    normed = (
        updated_wide
        * lax.rsqrt(jnp.mean(updated_wide * updated_wide, axis=-1, keepdims=True) + epsilon)
        * norm_gain
    ).astype(jnp.bfloat16)
    shared_expert_hidden = (
        jax.nn.silu(jnp.dot(normed, shared_gate, preferred_element_type=jnp.float32))
        * jnp.dot(normed, shared_up, preferred_element_type=jnp.float32)
    ).astype(jnp.bfloat16)
    shared = jnp.dot(shared_expert_hidden, shared_down, preferred_element_type=jnp.float32)
    expert_count = lax.axis_size(SP) * lax.axis_size("tp")
    top_count = routes.shape[1]
    capacity = own_rows * top_count * lax.axis_size("tp") // expert_count
    flat_expert = routes.reshape(own_rows * top_count)
    onehot = (flat_expert[:, None] == jnp.arange(expert_count, dtype=jnp.int32)[None, :]).astype(
        jnp.int32
    )
    position_in = jnp.sum(jnp.cumsum(onehot, axis=0) * onehot, axis=1) - 1
    slot_index = flat_expert * capacity + position_in
    source_row = jnp.arange(own_rows * top_count, dtype=jnp.int32) // top_count
    outgoing = (
        jnp.zeros((expert_count * capacity, model_width), jnp.bfloat16)
        .at[slot_index]
        .set(normed[source_row])
    )
    gate_matrix = w_gate[0]
    raising_projector = w_up[0]
    down_matrix = w_down[0]
    grouped = outgoing.reshape(lax.axis_size(SP), lax.axis_size("tp"), capacity, model_width)
    arrived = lax.all_to_all(
        lax.all_to_all(grouped, SP, split_axis=0, concat_axis=0, tiled=True),
        "tp",
        split_axis=1,
        concat_axis=1,
        tiled=True,
    )
    expert_arrived = arrived.reshape(expert_count, capacity, model_width)
    source_count, slot_count, width_now = expert_arrived.shape
    flat_rows = expert_arrived.reshape(source_count * slot_count, width_now)
    hidden = (
        jax.nn.silu(jnp.dot(flat_rows, gate_matrix, preferred_element_type=jnp.float32))
        * jnp.dot(flat_rows, raising_projector, preferred_element_type=jnp.float32)
    ).astype(jnp.bfloat16)
    answer = jnp.dot(hidden, down_matrix, preferred_element_type=jnp.float32).astype(jnp.bfloat16)
    answered = answer.reshape(source_count, slot_count, width_now).reshape(grouped.shape)
    returned = lax.all_to_all(
        lax.all_to_all(answered, SP, split_axis=0, concat_axis=0, tiled=True),
        "tp",
        split_axis=1,
        concat_axis=1,
        tiled=True,
    )
    results = returned.reshape(expert_count * capacity, model_width)[slot_index]
    results = results.reshape(own_rows, top_count, model_width)
    routed = jnp.sum(results.astype(jnp.float32) * route_weight[:, :, None], axis=1)
    return (updated_wide + shared + routed).astype(jnp.bfloat16)


def solution(mesh):
    finer = Mesh(mesh.devices.reshape(4, 4, 4, mesh.shape["tp"]), ("sp_0", "sp_1", "sp_2", "tp"))
    return jax.shard_map(
        local,
        mesh=finer,
        in_specs=(
            P(SP_TP, None),
            P(SP, "tp"),
            P(SP, "tp"),
            P(SP, "tp"),
            P(SP, "tp"),
            P(None, SP, "tp"),
            P(None, SP, "tp"),
            P("tp"),
            P("tp", None),
            P(),
            P(),
            P(),
            P(),
            P(SP_TP, None, None),
            P(SP_TP, None, None),
            P(SP_TP, None, None),
            P(SP_TP, None),
            P(SP_TP, None),
        ),
        out_specs=P(SP_TP, None),
        check_vma=False,
    )
```

profile of v0, /device:TPU:1, one launch (start us, length us, event | category | flops | bytes accessed | tf_op | source)
XLA Modules:
  0.0 442.6 jit_solution(16484694220752687930)
XLA Ops:
  13.0 8.3 %rev.21 = bf16[256,4,256]{2,0,1:T(8,128)(2,1)} reverse(bf16[256,4,256]{2,0,1:T(8,128)(2,1)} %bitcast.1185), dimensions={0} | reverse | bytes 1048576 | tf_op jit(solution)/shard_map/rev | solution.py:98
  28.9 8.5 %all-gather.9 = f32[4,1,4]{2,1,0:T(1,128)S(1)} all-gather(f32[1,1,4]{2,1,0:T(1,128)S(1)} %bitcast.1232), channel_id=1, replica_groups=mesh['sp_0'=4,'sp_1'=4,'sp_2'=4,'tp'=2] {'sp_2'}, dimensions={0}, use_global_device_ids=true | all-gather | bytes 80 | tf_op jit(solution)/shard_map/all_gather | solution.py:28
  39.0 7.2 %all-reduce.6 = f32[16]{0:T(128)S(1)} all-reduce(f32[16]{0:T(128)S(1)} %dynamic-update-slice), channel_id=5, replica_groups=mesh['sp_0'=4,'sp_1'=4,'sp_2'=4,'tp'=2] {'sp_2'}, use_global_device_ids=true, to_apply=%add.6 | all-reduce | flops 16 | bytes 128
  46.3 8.8 %all-gather.10 = f32[4,1,4]{2,1,0:T(1,128)S(1)} all-gather(f32[1,1,4]{2,1,0:T(1,128)S(1)} %get-tuple-element.175), channel_id=1, replica_groups=mesh['sp_0'=4,'sp_1'=4,'sp_2'=4,'tp'=2] {'sp_1'}, dimensions={0}, use_global_device_ids=true | all-gather | bytes 80 | tf_op jit(solution)/shard_map/all_gather | solution.py:28
  55.0 5.6 %all-gather.12 = f32[4,1,4]{2,1,0:T(1,128)S(1)} all-gather(f32[1,1,4]{2,1,0:T(1,128)S(1)} %get-tuple-element.174), channel_id=1, replica_groups=mesh['sp_0'=4,'sp_1'=4,'sp_2'=4,'tp'=2] {'sp_1'}, dimensions={0}, use_global_device_ids=true | all-gather | bytes 80 | tf_op jit(solution)/shard_map/all_gather | solution.py:28
  60.7 8.6 %all-gather.11 = f32[4,1,4]{2,1,0:T(1,128)S(1)} all-gather(f32[1,1,4]{2,1,0:T(1,128)S(1)} %get-tuple-element.173), channel_id=1, replica_groups=mesh['sp_0'=4,'sp_1'=4,'sp_2'=4,'tp'=2] {'sp_0'}, dimensions={0}, use_global_device_ids=true | all-gather | bytes 80 | tf_op jit(solution)/shard_map/all_gather | solution.py:28
  69.2 5.6 %all-gather.13 = f32[4,1,4]{2,1,0:T(1,128)S(1)} all-gather(f32[1,1,4]{2,1,0:T(1,128)S(1)} %get-tuple-element.172), channel_id=1, replica_groups=mesh['sp_0'=4,'sp_1'=4,'sp_2'=4,'tp'=2] {'sp_0'}, dimensions={0}, use_global_device_ids=true | all-gather | bytes 80 | tf_op jit(solution)/shard_map/all_gather | solution.py:28
  76.7 2.6 fusion.50
  79.4 10.8 %all-gather.28.cloned.1.call-done = f32[4,516,256]{2,1,0:T(8,128)} async-done(((f32[1,516,256]{2,1,0:T(8,128)}), f32[4,516,256]{2,1,0:T(8,128)}) %all-gather.28.cloned.1.call-update) | async-done | bytes 2113552 | tf_op jit(solution)/shard_map/all_gather | solution.py:46
  99.0 8.5 %all-gather.14 = f32[4,4,128]{2,1,0:T(4,128)S(1)} all-gather(f32[1,4,128]{2,1,0:T(4,128)S(1)} %bitcast.1227), channel_id=7, replica_groups=mesh['sp_0'=4,'sp_1'=4,'sp_2'=4,'tp'=2] {'sp_2'}, dimensions={0}, use_global_device_ids=true | all-gather | bytes 10240 | tf_op jit(solution)/shard_map/all_gather | solution.py:28
  108.2 9.6 %all_gather.90 = f32[4,4,128]{2,1,0:T(4,128)S(1)} all-gather(f32[1,4,128]{2,1,0:T(4,128)S(1)} %multiply_add_fusion.2), channel_id=1, replica_groups=mesh['sp_0'=4,'sp_1'=4,'sp_2'=4,'tp'=2] {'sp_1'}, dimensions={0}, use_global_device_ids=true | all-gather | bytes 10240 | tf_op jit(solution)/shard_map/all_gather | solution.py:28
  125.8 29.7 %all-gather.30.cloned.1.call-done = f32[4,516,256]{2,1,0:T(8,128)} async-done(((f32[1,516,256]{2,1,0:T(8,128)}), f32[4,516,256]{2,1,0:T(8,128)}) %all-gather.30.cloned.1.call-update) | async-done | bytes 2113552 | tf_op jit(solution)/shard_map/all_gather | solution.py:46
  170.5 10.1 %all_gather.91 = f32[4,4,128]{2,1,0:T(4,128)S(1)} all-gather(f32[1,4,128]{2,1,0:T(4,128)S(1)} %copy-done.52), channel_id=1, replica_groups=mesh['sp_0'=4,'sp_1'=4,'sp_2'=4,'tp'=2] {'sp_0'}, dimensions={0}, use_global_device_ids=true | all-gather | bytes 10240 | tf_op jit(solution)/shard_map/all_gather | solution.py:28
  188.0 2.9 fusion.407
  191.8 2.9 fusion.405
  194.8 4.5 %fusion.17 = f32[256,4,256]{0,2,1:T(8,128)S(1)} fusion(bf16[256,4,128]{2,0,1:T(8,128)(2,1)S(1)} %copy-done.10, f32[4,4,128,256]{3,2,1,0:T(8,128)} %all-gather.24.cloned.1.call-done, f32[256,4]{0,1:T(4,128)S(1)} %get-tuple-element.100, f32[4,4,128,256]{3,2,1,0:T(8,128)} %all-gather.22.cloned.1.call-done, f32[16,128,256]{2,1,0:T(8,128)} %all-gather.26.cloned.1.call-done, ...), kind=kOutput, calls=%fused_computation.29 | convolution fusion | flops 409862144 | bytes 7606764 | tf_op jit(solution)/shard_map/thd,hde->hte/dot_general | solution.py:139
  201.0 9.4 %rev.23 = f32[256,4,256]{0,2,1:T(8,128)} reverse(f32[256,4,256]{0,2,1:T(8,128)} %fusion.16), dimensions={0} | reverse | bytes 2097152 | tf_op jit(solution)/shard_map/rev | solution.py:151
  210.4 10.3 %all-gather.32.cloned.1.call-done = f32[4,516,256]{2,1,0:T(8,128)} async-done(((f32[1,516,256]{2,1,0:T(8,128)}), f32[4,516,256]{2,1,0:T(8,128)}) %all-gather.32.cloned.1.call-update) | async-done | bytes 2113552 | tf_op jit(solution)/shard_map/all_gather | solution.py:46
  230.2 4.0 convolution_convert_fusion.1
  234.2 5.4 %all_to_all.25 = bf16[2,128,2048]{2,1,0:T(8,128)(2,1)S(1)} all-to-all(bf16[2,128,2048]{2,1,0:T(8,128)(2,1)S(1)} %bitcast.1187), channel_id=1, replica_groups=mesh['sp_0'=4,'sp_1'=4,'sp_2'=4,'tp'=2] {'tp'}, dimensions={0} | all-to-all | bytes 2097152 | tf_op jit(solution)/shard_map/all_to_all | solution.py:77
  240.5 13.4 %scatter_custom_fusion = bf16[1024,2048]{1,0:T(8,128)(2,1)} fusion(s32[512]{0:T(512)S(1)} %bitcast.1228, bf16[128,2048]{1,0:T(8,128)(2,1)S(1)} %fusion.24, s32[1024]{0:T(1024)} %pad_clamp_fusion.1, bf16[]{:T(256)} %constant.84.clone.1), kind=kCustom, calls=%fused_computation.14 | custom fusion | bytes 4194816 | tf_op jit(solution)/shard_map/scatter | solution.py:228
  253.9 60.2 %all_to_all.26 = bf16[64,2,8,2048]{3,2,1,0:T(8,128)(2,1)S(1)} all-to-all(bf16[64,2,8,2048]{3,2,1,0:T(8,128)(2,1)} %bitcast.1176), channel_id=1, replica_groups=mesh['sp_0'=4,'sp_1'=4,'sp_2'=4,'tp'=2] {'sp_0','sp_1','sp_2'}, dimensions={0} | all-to-all | bytes 8388608 | tf_op jit(solution)/shard_map/all_to_all | solution.py:235
  314.7 8.7 %all_to_all.27 = bf16[64,2,8,2048]{3,2,0,1:T(8,128)(2,1)S(1)} all-to-all(bf16[64,2,8,2048]{3,2,0,1:T(8,128)(2,1)S(1)} %copy.158), channel_id=1, replica_groups=mesh['sp_0'=4,'sp_1'=4,'sp_2'=4,'tp'=2] {'tp'}, dimensions={1} | all-to-all | bytes 8388608 | tf_op jit(solution)/shard_map/all_to_all | solution.py:234
  326.0 3.6 fusion.3
  329.6 10.1 %convolution_convert_fusion = bf16[1024,2048]{1,0:T(8,128)(2,1)} fusion(bf16[1,512,2048]{2,1,0:T(8,128)(2,1)S(1)} %copy-done, f32[1024,512]{1,0:T(8,128)} %fusion.3, bf16[1024,2048]{1,0:T(8,128)(2,1)} %bitcast.1179, bf16[1,2048,512]{2,1,0:T(8,128)(2,1)} %param.31), kind=kOutput, calls=%fused_computation.4 | convolution fusion | flops 4300210176 | bytes 14680064 | tf_op jit(solution)/shard_map/dot_general | solution.py:248
  339.7 5.8 %all-to-all-start.3 = ((bf16[64,2,8,2048]{3,2,1,0:T(8,128)(2,1)}), bf16[64,2,8,2048]{3,2,1,0:T(8,128)(2,1)}, u32[]{:S(2)}, u32[]{:S(2)}) async-start(bf16[64,2,8,2048]{3,2,1,0:T(8,128)(2,1)} %bitcast.1177), calls=%async_computation.3 | async-start | bytes 8388608 | tf_op jit(solution)/shard_map/all_to_all | solution.py:251
  347.7 51.2 %all-to-all-done.3 = bf16[64,2,8,2048]{3,2,1,0:T(8,128)(2,1)} async-done(((bf16[64,2,8,2048]{3,2,1,0:T(8,128)(2,1)}), bf16[64,2,8,2048]{3,2,1,0:T(8,128)(2,1)}, u32[]{:S(2)}, u32[]{:S(2)}) %all-to-all-start.3) | async-done | bytes 4194336 | tf_op jit(solution)/shard_map/all_to_all | solution.py:251
  401.5 8.5 %all_to_all.28 = bf16[64,2,8,2048]{3,2,0,1:T(8,128)(2,1)S(1)} all-to-all(bf16[64,2,8,2048]{3,2,0,1:T(8,128)(2,1)S(1)} %copy.160), channel_id=1, replica_groups=mesh['sp_0'=4,'sp_1'=4,'sp_2'=4,'tp'=2] {'tp'}, dimensions={1} | all-to-all | bytes 8388608 | tf_op jit(solution)/shard_map/all_to_all | solution.py:250
  412.2 8.0 %gather_fusion = bf16[512,2048]{1,0:T(8,128)(2,1)} fusion(bf16[1024,2048]{1,0:T(8,128)(2,1)} %bitcast.1175, s32[1024]{0:T(1024)S(1)} %pad_clamp_fusion), kind=kCustom, calls=%fused_computation.1 | custom fusion | bytes 4196352 | tf_op jit(solution)/shard_map/gather | solution.py:257
  420.2 4.8 %reshape.4488 = f32[128,4,2048]{2,1,0:T(4,128)} reshape(bf16[512,2048]{1,0:T(8,128)(2,1)} %gather_fusion) | data formatting | bytes 6291456 | tf_op jit(solution)/shard_map/convert_element_type | solution.py:259
  425.0 6.4 %multiply_reduce_fusion = f32[128,2048]{1,0:T(8,128)} fusion(f32[128,4,2048]{2,1,0:T(4,128)} %reshape.4488, f32[128,4]{1,0:T(8,128)S(1)} %copy.162), kind=kLoop, calls=%fused_computation.3 | loop fusion | flops 1835008 | bytes 5244928 | tf_op jit(solution)/shard_map/reduce_sum | solution.py:259
  431.3 4.2 fusion.1
  (459 shorter events, 78.4 us)
Async XLA Ops:
  6.5 323.1 %copy-start = (bf16[1,512,2048]{2,1,0:T(8,128)(2,1)S(1)}, bf16[1,512,2048]{2,1,0:T(8,128)(2,1)}, u32[]{:S(2)}) copy-start(bf16[1,512,2048]{2,1,0:T(8,128)(2,1)} %param.33) | copy-start | bytes 6291460
  6.5 70.2 %all-gather.26.cloned.1.call-start = ((), (), s32[]{:S(2)}) async-start(), calls=%async_computation.7 | async-start | bytes 2621440 | tf_op jit(solution)/shard_map/all_gather | solution.py:28
  23.5 51.4 %copy-start.53 = (s32[128,4]{0,1:T(4,128)S(1)}, s32[128,4]{0,1:T(4,128)}, u32[]{:S(2)}) copy-start(s32[128,4]{0,1:T(4,128)} %param.34) | copy-start | bytes 6148
  23.5 66.7 %all-gather.28.cloned.1.call-start = ((), (), s32[]{:S(2)}) async-start(), calls=%async_computation.8 | async-start | bytes 2662400 | tf_op jit(solution)/shard_map/all_gather | solution.py:46
  28.8 94.3 %all-gather.22.cloned.1.call-start = ((), (), s32[]{:S(2)}) async-start(), calls=%async_computation.5 | async-start | bytes 2621440 | tf_op jit(solution)/shard_map/all_gather | solution.py:28
  76.7 30.8 %copy-start.22 = (f32[4]{0:T(128)}, f32[4]{0:T(128)S(1)}, u32[]{:S(2)}) copy-start(f32[4]{0:T(128)S(1)} %get-tuple-element.149) | copy-start | bytes 52
  79.3 76.1 %all-gather.30.cloned.1.call-start = ((), (), s32[]{:S(2)}) async-start(), calls=%async_computation.9 | async-start | bytes 2662400 | tf_op jit(solution)/shard_map/all_gather | solution.py:46
  97.7 96.9 %all-gather.24.cloned.1.call-start = ((), (), s32[]{:S(2)}) async-start(), calls=%async_computation.6 | async-start | bytes 2621440 | tf_op jit(solution)/shard_map/all_gather | solution.py:28
  121.4 34.9 %copy-start.37 = (f32[4]{0:T(128)}, f32[4]{0:T(128)S(1)}, u32[]{:S(2)}) copy-start(f32[4]{0:T(128)S(1)} %get-tuple-element.119) | copy-start | bytes 52
  121.4 41.4 %copy-start.35 = (f32[4]{0:T(128)}, f32[4]{0:T(128)S(1)}, u32[]{:S(2)}) copy-start(f32[4]{0:T(128)S(1)} %get-tuple-element.118) | copy-start | bytes 52
  121.4 41.4 %copy-start.39 = (f32[4]{0:T(128)}, f32[4]{0:T(128)S(1)}, u32[]{:S(2)}) copy-start(f32[4]{0:T(128)S(1)} %get-tuple-element.143) | copy-start | bytes 52
  121.4 41.4 %copy-start.41 = (f32[4]{0:T(128)}, f32[4]{0:T(128)S(1)}, u32[]{:S(2)}) copy-start(f32[4]{0:T(128)S(1)} %get-tuple-element.144) | copy-start | bytes 52
  121.5 41.4 %copy-start.43 = (f32[4]{0:T(128)}, f32[4]{0:T(128)S(1)}, u32[]{:S(2)}) copy-start(f32[4]{0:T(128)S(1)} %get-tuple-element.145) | copy-start | bytes 52
  121.5 41.4 %copy-start.45 = (f32[4]{0:T(128)}, f32[4]{0:T(128)S(1)}, u32[]{:S(2)}) copy-start(f32[4]{0:T(128)S(1)} %get-tuple-element.146) | copy-start | bytes 52
  121.5 41.4 %copy-start.47 = (f32[4]{0:T(128)}, f32[4]{0:T(128)S(1)}, u32[]{:S(2)}) copy-start(f32[4]{0:T(128)S(1)} %get-tuple-element.147) | copy-start | bytes 52
  121.5 41.4 %copy-start.49 = (f32[4]{0:T(128)}, f32[4]{0:T(128)S(1)}, u32[]{:S(2)}) copy-start(f32[4]{0:T(128)S(1)} %get-tuple-element.148) | copy-start | bytes 52
  125.7 94.9 %all-gather.32.cloned.1.call-start = ((), (), s32[]{:S(2)}) async-start(), calls=%async_computation.10 | async-start | bytes 2662400 | tf_op jit(solution)/shard_map/all_gather | solution.py:46
  200.8 21.7 %copy-start.60 = (f32[4]{0:T(128)S(1)}, f32[4]{0:T(128)}, u32[]{:S(2)}) copy-start(f32[4]{0:T(128)} %copy-done.59) | copy-start | bytes 52
  200.8 21.7 %copy-start.62 = (f32[4]{0:T(128)S(1)}, f32[4]{0:T(128)}, u32[]{:S(2)}) copy-start(f32[4]{0:T(128)} %copy-done.61) | copy-start | bytes 52
  200.8 21.7 %copy-start.64 = (f32[4]{0:T(128)S(1)}, f32[4]{0:T(128)}, u32[]{:S(2)}) copy-start(f32[4]{0:T(128)} %copy-done.63) | copy-start | bytes 52
  200.9 21.7 %copy-start.66 = (f32[4]{0:T(128)S(1)}, f32[4]{0:T(128)}, u32[]{:S(2)}) copy-start(f32[4]{0:T(128)} %copy-done.65) | copy-start | bytes 52
  200.9 21.7 %copy-start.68 = (f32[4]{0:T(128)S(1)}, f32[4]{0:T(128)}, u32[]{:S(2)}) copy-start(f32[4]{0:T(128)} %copy-done.67) | copy-start | bytes 52
  200.9 21.7 %copy-start.70 = (f32[4]{0:T(128)S(1)}, f32[4]{0:T(128)}, u32[]{:S(2)}) copy-start(f32[4]{0:T(128)} %copy-done.69) | copy-start | bytes 52
  200.9 21.7 %copy-start.72 = (f32[4]{0:T(128)S(1)}, f32[4]{0:T(128)}, u32[]{:S(2)}) copy-start(f32[4]{0:T(128)} %copy-done.71) | copy-start | bytes 52
  200.9 21.7 %copy-start.74 = (f32[4]{0:T(128)S(1)}, f32[4]{0:T(128)}, u32[]{:S(2)}) copy-start(f32[4]{0:T(128)} %copy-done.73) | copy-start | bytes 52
  200.9 21.7 %copy-start.76 = (f32[4]{0:T(128)S(1)}, f32[4]{0:T(128)}, u32[]{:S(2)}) copy-start(f32[4]{0:T(128)} %copy-done.75) | copy-start | bytes 52
  200.9 21.7 %copy-start.78 = (f32[4]{0:T(128)S(1)}, f32[4]{0:T(128)}, u32[]{:S(2)}) copy-start(f32[4]{0:T(128)} %copy-done.77) | copy-start | bytes 52
  200.9 21.7 %copy-start.80 = (f32[4]{0:T(128)S(1)}, f32[4]{0:T(128)}, u32[]{:S(2)}) copy-start(f32[4]{0:T(128)} %copy-done.79) | copy-start | bytes 52
  200.9 21.7 %copy-start.82 = (f32[4]{0:T(128)S(1)}, f32[4]{0:T(128)}, u32[]{:S(2)}) copy-start(f32[4]{0:T(128)} %copy-done.81) | copy-start | bytes 52
  200.9 21.7 %copy-start.84 = (f32[4]{0:T(128)S(1)}, f32[4]{0:T(128)}, u32[]{:S(2)}) copy-start(f32[4]{0:T(128)} %copy-done.83) | copy-start | bytes 52
  201.0 21.9 %copy-start.7 = (bf16[256,512]{1,0:T(8,128)(2,1)S(1)}, bf16[256,512]{1,0:T(8,128)(2,1)}, u32[]{:S(2)}) copy-start(bf16[256,512]{1,0:T(8,128)(2,1)} %param.19) | copy-start | bytes 786436
  339.7 59.2 %all-to-all-start.3 = ((bf16[64,2,8,2048]{3,2,1,0:T(8,128)(2,1)}), bf16[64,2,8,2048]{3,2,1,0:T(8,128)(2,1)}, u32[]{:S(2)}, u32[]{:S(2)}) async-start(bf16[64,2,8,2048]{3,2,1,0:T(8,128)(2,1)} %bitcast.1177), calls=%async_computation.3 | async-start | bytes 8388608 | tf_op jit(solution)/shard_map/all_to_all | solution.py:251
  (93 other events, 652.2 us)
Sparse Core Ops, SparseCore 0:
  23.6 33.9 all-gather.25
  59.2 30.9 all-gather.27
  91.9 31.0 all-gather.21
  124.5 30.9 all-gather.29
  157.0 31.1 all-gather.23
  189.6 30.9 all-gather.31
where the time goes:
time: 451 us; the launch traced here: 443 us
  blocking collectives  155 us (34%)
  waiting for transfers between devices  102 us (23%)
  local copies, waits for them, and re-layouts  86.5 us (19%)
  matrix products  39.3 us (9%)
  other arithmetic  37.3 us (8%)
  between operations  16.2 us (4%)
  starting transfers between devices  6.02 us (1%)
    all_gather x8, blocking collectives, prefix_by_axis(): pieces = jax.tree.map(lambda part: lax.all_gather(part, axis), total)  65.3 us
    all_to_all x1, blocking collectives, local(): lax.all_to_all(grouped, SP, split_axis=0, concat_axis=0, tiled=True)  60.2 us
    all_to_all x1, waiting for transfers between devices, local(): lax.all_to_all(answered, SP, split_axis=0, concat_axis=0, tiled=True)  51.2 us
    all_gather x3, waiting for transfers between devices, gathered_once(): both, at, found = (lax.all_gather(jnp.concatenate(lines), axis), 0, {})  50.8 us
    scatter x1, local copies, waits for them, and re-layouts, local(): outgoing = jnp.zeros((expert_count * capacity, model_width), jnp.bfloat16...  13.4 us
    dot_general x1, matrix products, local(): jnp.dot(hidden, down_matrix, preferred_element_type=jnp.float32)  10.1 us
    rev x1, local copies, waits for them, and re-layouts, cell_direction(): result = result[::-1]  9.4 us
    add x4, other arithmetic, combine_states(): early_scale[:, None, None] * early_matrix  9.2 us
  transfers between devices with their start and end apart: 7, of which 4 were waited for; matrix products, arithmetic and copies ran while one was open for 16% of the time, Pallas kernels for 0%

commit v1 on v0

v1 whole, which is shorter than its diff:
```python
import functools
import math

import jax
import jax.numpy as jnp
from jax import lax
from jax.experimental import pallas as pl
from jax.experimental.pallas import tpu as pltpu
from jax.sharding import Mesh
from jax.sharding import PartitionSpec as P

SP = ("sp_0", "sp_1", "sp_2")
SP_TP = ("sp_0", "sp_1", "sp_2", "tp")
MESH = pl.DeviceIdType.MESH

epsilon = 1e-06
max_floor = -1e30
f32 = jnp.float32
bf16 = jnp.bfloat16

NT = (((1,), (1,)), ((), ()))
TN = (((0,), (0,)), ((), ()))
NN = (((1,), (0,)), ((), ()))


def exact(a, b, dims):
    return lax.dot_general(
        a, b, dims, precision=lax.Precision.HIGHEST, preferred_element_type=f32
    )


def mul(a, b, dims=NN):
    return lax.dot_general(a, b, dims, preferred_element_type=f32)


def here():
    return tuple(lax.axis_index(a) for a in SP_TP)


def spots():
    return tuple(lax.axis_size(a) for a in SP_TP)


def flat(at, sizes):
    number = at[0]
    for part, size in zip(at[1:], sizes[1:]):
        number = number * size + part
    return number


def away(step, sign):
    at, sizes = here(), spots()
    out = []
    rest = step
    for part, size in reversed(list(zip(at, sizes))):
        move = lax.rem(rest, size)
        rest = rest // size
        out.append(lax.rem(part + (move if sign > 0 else size - move), size))
    return tuple(reversed(out))


def mixer_kernel(
    heads,
    key_dim,
    value_dim,
    gates_ref,
    gain_ref,
    norm_gain_ref,
    q_hbm,
    k_hbm,
    v_hbm,
    og_hbm,
    res_hbm,
    wout_hbm,
    updated_ref,
    normed_ref,
    q,
    k,
    v,
    og,
    res,
    wout,
    out_m,
    in_m,
    back_m,
    state_m,
    out_a,
    in_a,
    back_a,
    state_a,
    local,
    mixed,
    proj_out,
    proj_in,
    proj_own,
    load_sem,
    send_sem,
    recv_sem,
    pair_sem,
):
    sizes = spots()
    places = sizes[0] * sizes[1] * sizes[2]
    z, y, x, core = here()
    me = flat((z, y, x), sizes[:3])
    rows = q.shape[0]
    units = 2 * heads
    chunks = places // units
    piece = out_m.shape[1]
    key_scale = 1.0 / math.sqrt(key_dim)

    loads = [
        pltpu.make_async_copy(a, b, load_sem.at[n])
        for n, (a, b) in enumerate(
            [(k_hbm, k), (v_hbm, v), (q_hbm, q), (og_hbm, og), (res_hbm, res), (wout_hbm, wout)]
        )
    ]
    for load in loads:
        load.start()

    barrier = pltpu.get_barrier_semaphore()
    two = sizes[3]

    def greet(step, carry):
        pl.semaphore_signal(barrier, inc=1, device_id=away(step * two, 1), device_id_type=MESH)
        return carry

    lax.fori_loop(1, places, greet, 0)
    partner = (z, y, x, lax.rem(core + 1, two))
    pl.semaphore_signal(barrier, inc=1, device_id=partner, device_id_type=MESH)

    ig = gates_ref[0:units, :]
    decay = jnp.exp(-gates_ref[units : 2 * units, :])
    up = 1.0 + decay
    lf = -jnp.where(up == 1.0, decay, jnp.log(up) * (decay / jnp.where(up == 1.0, 1.0, up - 1.0)))

    line = lax.broadcasted_iota(jnp.int32, (rows, rows), 0)
    lane = lax.broadcasted_iota(jnp.int32, (rows, rows), 1)
    upper = (line <= lane).astype(f32)
    lower = (line >= lane).astype(f32)
    eye = (line == lane).astype(f32)
    first_row = lax.broadcasted_iota(jnp.int32, (units, rows), 0) < heads
    first_col = lax.broadcasted_iota(jnp.int32, (rows, units), 1) < heads
    run_row = jnp.where(first_row, exact(lf, upper, NN), exact(lf, lower, NN))
    run_col = jnp.where(first_col, exact(lower, lf, NT), exact(upper, lf, NT))
    ig_col = exact(eye, ig, NT)
    total_col = jnp.where(first_col[0:1], run_col[rows - 1 : rows, :], run_col[0:1, :])
    a_col = total_col - run_col + ig_col
    peak_col = jnp.max(a_col, axis=0, keepdims=True)
    scale_col = jnp.exp(a_col - peak_col) * key_scale

    loads[0].wait()
    loads[1].wait()
    for unit in range(units):
        h = unit % heads
        kh = k[:, h * key_dim : (h + 1) * key_dim].astype(f32)
        low = (kh * scale_col[:, unit : unit + 1]).astype(bf16)
        matrix = mul(low, v[:, h * value_dim : (h + 1) * value_dim], TN)
        out_m[unit * chunks : (unit + 1) * chunks] = matrix.astype(bf16).reshape(
            chunks, piece, value_dim
        )
        norm = jnp.sum(low.astype(f32), axis=0, keepdims=True)
        out_a[unit, 0:1, :] = norm
        out_a[unit, 1:2, :] = jnp.broadcast_to(peak_col[:, unit : unit + 1], (1, key_dim))
        out_a[unit, 2:3, :] = jnp.broadcast_to(total_col[:, unit : unit + 1], (1, key_dim))

    pl.semaphore_wait(barrier, places)

    def exchange(round_at, src_m, dst_m, src_a, dst_a, a_of):
        def copies(step, sign):
            other = away(step * two, sign)
            spot = flat(other[:3], sizes[:3])
            return [
                pltpu.make_async_remote_copy(
                    src_ref=src_m.at[spot],
                    dst_ref=dst_m.at[me],
                    send_sem=send_sem.at[round_at, 0, step],
                    recv_sem=recv_sem.at[round_at, 0, step],
                    device_id=other,
                    device_id_type=MESH,
                ),
                pltpu.make_async_remote_copy(
                    src_ref=src_a.at[a_of(spot)],
                    dst_ref=dst_a.at[me],
                    send_sem=send_sem.at[round_at, 1, step],
                    recv_sem=recv_sem.at[round_at, 1, step],
                    device_id=other,
                    device_id_type=MESH,
                ),
            ]

        def go(i, carry):
            for copy in copies(lax.rem(i * 27, places), 1):
                copy.start()
            return carry

        lax.fori_loop(1, places, go, 0)
        dst_m[me] = src_m[me]
        dst_a[me] = src_a[a_of(me)]

        def finish(i, carry):
            step = lax.rem(i * 27, places)
            source = away(step * two, -1)
            spot = flat(source[:3], sizes[:3])
            pltpu.make_async_copy(
                src_m.at[spot], dst_m.at[spot], recv_sem.at[round_at, 0, step]
            ).wait()
            pltpu.make_async_copy(
                src_a.at[a_of(spot)], dst_a.at[spot], recv_sem.at[round_at, 1, step]
            ).wait()
            for copy in copies(step, 1):
                copy.wait_send()
            return carry

        return lambda: lax.fori_loop(1, places, finish, 0)

    arrive = exchange(0, out_m, in_m, out_a, in_a, lambda spot: spot // chunks)

    loads[2].wait()
    peaks, sums = [], []
    for h in range(heads):
        qh = q[:, h * key_dim : (h + 1) * key_dim]
        kh = k[:, h * key_dim : (h + 1) * key_dim]
        vh = v[:, h * value_dim : (h + 1) * value_dim]
        scores = mul(qh, kh, NT) * key_scale
        for way in range(2):
            unit = way * heads + h
            seen = (line >= lane) if way == 0 else (line <= lane)
            pair = run_col[:, unit : unit + 1] + (ig[unit : unit + 1] - run_row[unit : unit + 1])
            pair = jnp.where(seen, pair, max_floor)
            top = jnp.max(pair, axis=1, keepdims=True)
            weight = jnp.where(seen, jnp.exp(pair - top), 0.0) * scores
            local[unit] = mul(weight.astype(bf16), vh)
            peaks.append(top)
            sums.append(jnp.sum(weight, axis=1, keepdims=True))

    arrive()
    backward = me // (chunks * heads)

    def advance(s, carry):
        m, n, top = carry
        at = s + backward * (places - 1 - 2 * s)
        back_m[at] = m.astype(bf16)
        back_a[at, 0:1, :] = n
        back_a[at, 1:2, :] = top
        block_top = in_a[at, 1:2, :]
        moved = in_a[at, 2:3, :] + top
        new = jnp.maximum(moved, block_top)
        keep = jnp.exp(moved - new)
        add = jnp.exp(block_top - new)
        wide_keep = jnp.concatenate([keep] * (value_dim // key_dim), axis=1)
        wide_add = jnp.concatenate([add] * (value_dim // key_dim), axis=1)
        m = wide_keep * m + wide_add * in_m[at].astype(f32)
        n = keep * n + add * in_a[at, 0:1, :]
        return m, n, new

    lax.fori_loop(
        0,
        places,
        advance,
        (
            jnp.zeros((piece, value_dim), f32),
            jnp.zeros((1, key_dim), f32),
            jnp.full((1, key_dim), max_floor, f32),
        ),
    )
    arrive = exchange(1, back_m, state_m, back_a, state_a, lambda spot: spot)
    loads[3].wait()
    arrive()

    for h in range(heads):
        qh = q[:, h * key_dim : (h + 1) * key_dim]
        qw = qh.astype(f32)
        total = None
        for way in range(2):
            unit = way * heads + h
            state = state_m[unit * chunks : (unit + 1) * chunks].reshape(key_dim, value_dim)
            norm = state_a[unit * chunks, 0:1, :]
            top = state_a[unit * chunks, 1:2, :]
            crossing = run_col[:, unit : unit + 1] + top[:, 0:1]
            row_max = jnp.maximum(crossing, peaks[h * 2 + way])
            carry = jnp.exp(crossing - row_max)
            inner = jnp.exp(peaks[h * 2 + way] - row_max)
            read_norm = jnp.sum(qw * norm, axis=1, keepdims=True)
            divisor = carry * read_norm + inner * sums[h * 2 + way]
            divisor = jnp.maximum(jnp.abs(divisor), jnp.exp(-row_max))
            part = (carry * mul(qh, state) + inner * local[unit]) / divisor
            total = part if total is None else total + part
        normal = total * lax.rsqrt(jnp.mean(total * total, axis=1, keepdims=True) + epsilon)
        span = slice(h * value_dim, (h + 1) * value_dim)
        gate = 1.0 / (1.0 + jnp.exp(-og[:, span].astype(f32)))
        mixed[:, span] = (normal * gain_ref[:, span] * gate).astype(bf16)

    loads[4].wait()
    loads[5].wait()
    half = res.shape[0]
    width = res.shape[1]
    tile = 512
    theirs = pl.ds(pl.multiple_of((1 - core) * half, half), half)
    mine = pl.ds(pl.multiple_of(core * half, half), half)

    def project(n, carry, span, ref):
        cols = pl.ds(pl.multiple_of(n * tile, tile), tile)
        ref[:, cols] = mul(mixed[span, :], wout[:, cols]).astype(ref.dtype)
        return carry

    lax.fori_loop(0, width // tile, functools.partial(project, span=theirs, ref=proj_out), 0)
    trade = pltpu.make_async_remote_copy(
        src_ref=proj_out,
        dst_ref=proj_in,
        send_sem=pair_sem.at[0],
        recv_sem=pair_sem.at[1],
        device_id=partner,
        device_id_type=MESH,
    )
    trade.start()
    lax.fori_loop(0, width // tile, functools.partial(project, span=mine, ref=proj_own), 0)
    trade.wait()
    updated = (res[...].astype(f32) + (proj_own[...] + proj_in[...].astype(f32))).astype(bf16)
    updated_ref[...] = updated
    wide = updated.astype(f32)
    normed_ref[...] = (
        wide
        * lax.rsqrt(jnp.mean(wide * wide, axis=1, keepdims=True) + epsilon)
        * norm_gain_ref[...]
    ).astype(bf16)


def mixer(residual, queries, keys, values, out_gate, gates, head_gain, w_out, norm_gain):
    rows, query_width = queries.shape
    heads = gates.shape[0] // 4
    key_dim, value_dim = query_width // heads, values.shape[1] // heads
    places = math.prod(lax.axis_size(a) for a in SP)
    units = 2 * heads
    piece = key_dim * units // places
    half, width = residual.shape
    vmem = pl.BlockSpec(memory_space=pltpu.VMEM)
    hbm = pl.BlockSpec(memory_space=pl.ANY)
    matrices = pltpu.VMEM((places, piece, value_dim), bf16)
    extras = pltpu.VMEM((places, 4, key_dim), f32)
    return pl.pallas_call(
        functools.partial(mixer_kernel, heads, key_dim, value_dim),
        out_shape=[jax.ShapeDtypeStruct((half, width), bf16)] * 2,
        in_specs=[vmem] * 3 + [hbm] * 6,
        out_specs=[vmem] * 2,
        scratch_shapes=[
            pltpu.VMEM(queries.shape, bf16),
            pltpu.VMEM(keys.shape, bf16),
            pltpu.VMEM(values.shape, bf16),
            pltpu.VMEM(out_gate.shape, bf16),
            pltpu.VMEM(residual.shape, bf16),
            pltpu.VMEM(w_out.shape, bf16),
            matrices,
            matrices,
            matrices,
            matrices,
            pltpu.VMEM((units, 4, key_dim), f32),
            extras,
            extras,
            extras,
            pltpu.VMEM((units, rows, value_dim), f32),
            pltpu.VMEM(values.shape, bf16),
            pltpu.VMEM((half, width), bf16),
            pltpu.VMEM((half, width), bf16),
            pltpu.VMEM((half, width), f32),
            pltpu.SemaphoreType.DMA((6,)),
            pltpu.SemaphoreType.DMA((2, 2, places)),
            pltpu.SemaphoreType.DMA((2, 2, places)),
            pltpu.SemaphoreType.DMA((2,)),
        ],
        compiler_params=pltpu.CompilerParams(
            collective_id=0, has_side_effects=True, vmem_limit_bytes=48 * 1024 * 1024
        ),
        name="mixer",
    )(
        gates,
        head_gain.reshape(1, -1),
        norm_gain.reshape(1, -1),
        queries,
        keys,
        values,
        out_gate,
        residual,
        w_out,
    )


def silu(value):
    return value / (1.0 + jnp.exp(-value))


def experts_kernel(
    slots,
    group,
    stride,
    normed,
    updated,
    routes_row,
    routes_col,
    weight_col,
    sg_hbm,
    su_hbm,
    sd_hbm,
    wg_hbm,
    wu_hbm,
    wd_hbm,
    out_ref,
    sg,
    su,
    sd,
    wg,
    wu,
    wd,
    outgoing,
    arrived,
    returned,
    packed,
    answer,
    hidden,
    shared_hidden,
    total,
    load_sem,
    send_sem,
    recv_sem,
    send_back,
    recv_back,
):
    sizes = spots()
    count = math.prod(sizes)
    me = flat(here(), sizes)
    tokens, width = normed.shape
    top = routes_row.shape[0]
    tile = 512

    loads = [
        pltpu.make_async_copy(a, b, load_sem.at[n])
        for n, (a, b) in enumerate(
            [
                (sg_hbm, sg),
                (su_hbm, su),
                (sd_hbm, sd),
                (wg_hbm.at[0], wg),
                (wu_hbm.at[0], wu),
                (wd_hbm.at[0], wd),
            ]
        )
    ]
    for load in loads:
        load.start()

    barrier = pltpu.get_barrier_semaphore()

    def greet(step, carry):
        pl.semaphore_signal(barrier, inc=1, device_id=away(step, 1), device_id_type=MESH)
        return carry

    lax.fori_loop(1, count, greet, 0)

    expert = lax.broadcasted_iota(jnp.int32, (count, tokens), 0)
    named = jnp.zeros((count, tokens), f32)
    for n in range(top):
        named = named + (expert == routes_row[n : n + 1, :]).astype(f32)
    earlier = (
        lax.broadcasted_iota(jnp.int32, (tokens, tokens), 0)
        < lax.broadcasted_iota(jnp.int32, (tokens, tokens), 1)
    ).astype(bf16)
    rank = mul(named.astype(bf16), earlier)
    rank = jnp.where(named > 0.0, rank, -1.0)
    total[:, 0:tokens] = rank
    block = 16

    def fill(b, carry):
        lines = pl.ds(pl.multiple_of(b * block, block), block)
        at = total[lines, 0:tokens]
        slot = lax.broadcasted_iota(jnp.int32, (block, slots, tokens), 1).astype(f32)
        pick = (at[:, None, :] == slot).astype(f32).reshape(block * slots, tokens)
        moved = mul(pick.astype(bf16), normed[...])
        outgoing[lines] = moved.reshape(block, slots, width).astype(bf16)
        return carry

    lax.fori_loop(0, count // block, fill, 0)
    pl.semaphore_wait(barrier, count - 1)

    def dispatch(i):
        other = away(lax.rem(i * stride, count), 1)
        return pltpu.make_async_remote_copy(
            src_ref=outgoing.at[flat(other, sizes)],
            dst_ref=arrived.at[i],
            send_sem=send_sem.at[i],
            recv_sem=recv_sem.at[i],
            device_id=other,
            device_id_type=MESH,
        )

    def give_back(i):
        source = away(lax.rem(i * stride, count), -1)
        return pltpu.make_async_remote_copy(
            src_ref=answer.at[i],
            dst_ref=returned.at[me],
            send_sem=send_back.at[i],
            recv_sem=recv_back.at[i],
            device_id=source,
            device_id_type=MESH,
        )

    def send(i, carry):
        dispatch(i).start()
        return carry

    lax.fori_loop(1, count, send, 0)
    arrived[0] = outgoing[me]

    for load in loads[:3]:
        load.wait()
    shared_hidden[...] = (silu(mul(normed[...], sg[...])) * mul(normed[...], su[...])).astype(bf16)

    def shared_part(n, carry):
        cols = pl.ds(pl.multiple_of(n * tile, tile), tile)
        total[:, cols] = updated[:, cols].astype(f32) + mul(shared_hidden[...], sd[:, cols])
        return carry

    lax.fori_loop(0, width // tile, shared_part, 0)

    for load in loads[3:]:
        load.wait()

    def work(g, carry):
        def landed(i, inner):
            dispatch(i).wait_recv()
            return inner

        lax.fori_loop(jnp.maximum(g * group, 1), (g + 1) * group, landed, 0)
        sources = pl.ds(pl.multiple_of(g * group, group), group)
        packed[...] = arrived[sources].astype(f32).reshape(group * slots, width).astype(bf16)
        hidden[...] = (silu(mul(packed[...], wg[...])) * mul(packed[...], wu[...])).astype(bf16)

        def down(n, inner):
            cols = pl.ds(pl.multiple_of(n * tile, tile), tile)
            answer[sources, :, cols] = (
                mul(hidden[...], wd[:, cols]).reshape(group, slots, tile).astype(bf16)
            )
            return inner

        lax.fori_loop(0, width // tile, down, 0)

        def reply(i, inner):
            give_back(i).start()
            return inner

        lax.fori_loop(jnp.maximum(g * group, 1), (g + 1) * group, reply, 0)
        return carry

    lax.fori_loop(0, count // group, work, 0)
    returned[me] = answer[0]

    def close(i, carry):
        dispatch(i).wait_send()
        give_back(i).wait_send()
        give_back(i).wait_recv()
        return carry

    lax.fori_loop(1, count, close, 0)

    span = count * slots
    lane = lax.broadcasted_iota(jnp.int32, (tokens, span), 1)
    owner = lane // slots
    marks = jnp.zeros((tokens, span), f32)
    share = jnp.zeros((tokens, span), f32)
    for n in range(top):
        hit = owner == routes_col[:, n : n + 1]
        marks = marks + hit.astype(f32)
        share = share + jnp.where(hit, weight_col[:, n : n + 1], 0.0)
    before = (
        lax.broadcasted_iota(jnp.int32, (tokens, tokens), 1)
        < lax.broadcasted_iota(jnp.int32, (tokens, tokens), 0)
    ).astype(bf16)
    order = mul(before, marks.astype(bf16))
    share = jnp.where(order == (lane - owner * slots).astype(f32), share, 0.0)
    high = share.astype(bf16)
    low = (share - high.astype(f32)).astype(bf16)

    def gather(n, carry):
        cols = pl.ds(pl.multiple_of(n * tile, tile), tile)
        rows = returned[:, :, cols].astype(f32).reshape(span, tile).astype(bf16)
        out_ref[:, cols] = (total[:, cols] + (mul(high, rows) + mul(low, rows))).astype(bf16)
        return carry

    lax.fori_loop(0, width // tile, gather, 0)


def experts(normed, updated, routes, weight, shared_gate, shared_up, shared_down, gate, up, down):
    tokens, width = normed.shape
    top = routes.shape[1]
    count = math.prod(lax.axis_size(a) for a in SP_TP)
    slots = tokens * top * lax.axis_size("tp") // count
    group = 32
    hidden = gate.shape[2]
    vmem = pl.BlockSpec(memory_space=pltpu.VMEM)
    hbm = pl.BlockSpec(memory_space=pl.ANY)
    rows = pltpu.VMEM((count, slots, width), bf16)
    return pl.pallas_call(
        functools.partial(experts_kernel, slots, group, 37),
        out_shape=jax.ShapeDtypeStruct((tokens, width), bf16),
        in_specs=[vmem] * 5 + [hbm] * 6,
        out_specs=vmem,
        scratch_shapes=[
            pltpu.VMEM(shared_gate.shape, bf16),
            pltpu.VMEM(shared_up.shape, bf16),
            pltpu.VMEM(shared_down.shape, bf16),
            pltpu.VMEM(gate.shape[1:], bf16),
            pltpu.VMEM(up.shape[1:], bf16),
            pltpu.VMEM(down.shape[1:], bf16),
            rows,
            rows,
            rows,
            pltpu.VMEM((group * slots, width), bf16),
            rows,
            pltpu.VMEM((group * slots, hidden), bf16),
            pltpu.VMEM((tokens, shared_gate.shape[1]), bf16),
            pltpu.VMEM((tokens, width), f32),
            pltpu.SemaphoreType.DMA((6,)),
            pltpu.SemaphoreType.DMA((count,)),
            pltpu.SemaphoreType.DMA((count,)),
            pltpu.SemaphoreType.DMA((count,)),
            pltpu.SemaphoreType.DMA((count,)),
        ],
        compiler_params=pltpu.CompilerParams(
            collective_id=1, has_side_effects=True, vmem_limit_bytes=60 * 1024 * 1024
        ),
        name="experts",
    )(
        normed,
        updated,
        routes.T,
        routes,
        weight,
        shared_gate,
        shared_up,
        shared_down,
        gate,
        up,
        down,
    )


def local(
    residual,
    queries,
    keys,
    values,
    out_gate,
    in_gate,
    forget_gate,
    head_gain,
    w_out,
    norm_gain,
    shared_gate,
    shared_up,
    shared_down,
    w_gate,
    w_up,
    w_down,
    routes,
    route_weight,
):
    gates = jnp.stack([in_gate, forget_gate]).transpose(0, 1, 3, 2)
    gates = gates.reshape(-1, in_gate.shape[1])
    updated, normed = mixer(
        residual, queries, keys, values, out_gate, gates, head_gain, w_out, norm_gain
    )
    return experts(
        normed,
        updated,
        routes,
        route_weight,
        shared_gate,
        shared_up,
        shared_down,
        w_gate,
        w_up,
        w_down,
    )


def solution(mesh):
    finer = Mesh(mesh.devices.reshape(4, 4, 4, mesh.shape["tp"]), SP_TP)
    return jax.shard_map(
        local,
        mesh=finer,
        in_specs=(
            P(SP_TP, None),
            P(SP, "tp"),
            P(SP, "tp"),
            P(SP, "tp"),
            P(SP, "tp"),
            P(None, SP, "tp"),
            P(None, SP, "tp"),
            P("tp"),
            P("tp", None),
            P(),
            P(),
            P(),
            P(),
            P(SP_TP, None, None),
            P(SP_TP, None, None),
            P(SP_TP, None, None),
            P(SP_TP, None),
            P(SP_TP, None),
        ),
        out_specs=P(SP_TP, None),
        check_vma=False,
    )
```

time: 451 us -> 169 us (0.37); the launches traced: 443 us -> 169 us
  Pallas kernels: 0 us -> 155 us
  blocking collectives: 155 us -> 0 us
  waiting for transfers between devices: 102 us -> 0 us
  local copies, waits for them, and re-layouts: 86.5 us -> 12.7 us
  matrix products: 39.3 us -> 0 us
  other arithmetic: 37.3 us -> 0.72 us
  between operations: 16.2 us -> 0.04 us
  starting transfers between devices: 6.02 us -> 0 us
    pallas_call x0 -> x2, Pallas kernels: none -> 155 us  [the longest x1 110 us: experts(): pl.pallas_call(functools.partial(experts_kernel, slots, group, 37), out_s...]
    all_to_all x4 -> x0, blocking collectives: 82.7 us -> none  [the longest x1 60.2 us: local(): lax.all_to_all(grouped, SP, split_axis=0, concat_axis=0, tiled=True)]
    all_gather x8 -> x0, blocking collectives: 65.3 us -> none  [prefix_by_axis(): pieces = jax.tree.map(lambda part: lax.all_gather(part, axis), total)]
    all_to_all x1 -> x0, waiting for transfers between devices: 51.2 us -> none  [local(): lax.all_to_all(answered, SP, split_axis=0, concat_axis=0, tiled=True)]
    all_gather x6 -> x0, waiting for transfers between devices: 50.8 us -> none  [the longest x3 50.8 us: gathered_once(): both, at, found = (lax.all_gather(jnp.concatenate(lines), axis), 0, {})]
    dot_general x15 -> x0, matrix products: 39.3 us -> none  [the longest x1 10.1 us: local(): jnp.dot(hidden, down_matrix, preferred_element_type=jnp.float32)]
    rev x6 -> x0, local copies, waits for them, and re-layouts: 20.9 us -> none  [the longest x1 9.4 us: cell_direction(): result = result[::-1]]
    scatter x1 -> x0, local copies, waits for them, and re-layouts: 13.4 us -> none  [local(): outgoing = jnp.zeros((expert_count * capacity, model_width), jnp.bfloat16...]
  transfers between devices with their start and end apart: 7 -> 0, of which waited for: 4 -> 0; matrix products, arithmetic and copies ran while one was open for 16% -> 0% of each run, Pallas kernels for 0% -> 0%
where the time goes in v1:
time: 169 us
  Pallas kernels  155 us (92%)
  local copies, waits for them, and re-layouts  12.7 us (8%)
    pallas_call x1, Pallas kernels, experts(): pl.pallas_call(functools.partial(experts_kernel, slots, group, 37), out_s...  110 us
    pallas_call x1, Pallas kernels, mixer(): pl.pallas_call(functools.partial(mixer_kernel, heads, key_dim, value_dim)...  44.8 us
    unnamed x21, local copies, waits for them, and re-layouts  12.7 us

profile of v1, /device:TPU:1, one launch (start us, length us, event | category | flops | bytes accessed | tf_op | source)
XLA Modules:
  0.0 168.6 jit_solution(6388413342148708493)
XLA Ops:
  0.0 0.7 maximum_bitcast_fusion
  0.7 1.4 copy.20.weight_col
  2.1 1.4 copy.19.routes_col
  3.6 0.0 copy-start
  3.6 1.0 copy-done
  4.6 0.0 copy-start.1
  4.6 1.0 copy-done.1
  5.6 0.0 copy-start.2
  5.6 1.0 copy-done.2
  6.7 0.0 copy-start.5
  6.7 0.9 copy-done.5
  7.6 0.0 copy-start.6
  7.6 0.9 copy-done.6
  8.6 0.0 copy-start.7
  8.6 0.7 copy-done.7
  9.3 0.0 copy-start.8
  9.3 0.7 copy-done.8
  10.0 44.8 %mixer.1 = (bf16[128,2048]{1,0:T(8,128)(2,1)S(1)}, bf16[128,2048]{1,0:T(8,128)(2,1)S(1)}) custom-call(f32[16,256]{1,0:T(8,128)S(1)} %reshape.9.gates_ref, f32[1,1024]{1,0:T(1,128)S(1)} %bitcast.8, f32[1,2048]{1,0:T(1,128)S(1)} %bitcast.7, bf16[256,512]{1,0:T(8,128)(2,1)S(1)} %copy-done.5, bf16[256,512]{1,0:T(8,128)(2,1)S(1)} %copy-done.6, ...), custom_call_target="tpu_custom_call" | custom-call | tf_op jit(solution)/shard_map/mixer/pallas_call | solution.py:340
  54.8 0.0 copy-start.3
  54.8 0.8 copy-done.3
  55.6 0.0 copy-start.4
  55.6 0.8 copy-done.4
  56.4 110.3 %experts.1 = bf16[128,2048]{1,0:T(8,128)(2,1)} custom-call(bf16[128,2048]{1,0:T(8,128)(2,1)} %copy-done.4, bf16[128,2048]{1,0:T(8,128)(2,1)} %copy-done.3, s32[4,128]{1,0:T(4,128)} %bitcast.11, s32[128,4]{1,0:T(8,128)} %copy.19.routes_col, f32[128,4]{1,0:T(8,128)} %copy.20.weight_col, bf16[2048,512]{1,0:T(8,128)(2,1)} %sg_hbm.1, bf16[2048,512]{1,0:T(8,128)(2,1)} %su_hbm.1, ...), custom_call_target="tpu_custom_call" | custom-call | tf_op jit(solution)/shard_map/experts/pallas_call | solution.py:600
  166.7 1.9 %copy.22 = bf16[128,2048]{1,0:T(8,128)(2,1)} copy(bf16[128,2048]{1,0:T(8,128)(2,1)} %experts.1) | data formatting | bytes 1048576
  (1 shorter events, 0.0 us)
Async XLA Ops:
  3.6 1.0 copy-start
  4.6 1.0 copy-start.1
  5.6 1.0 copy-start.2
  6.7 0.9 copy-start.5
  7.6 0.9 copy-start.6
  8.6 0.7 copy-start.7
  9.3 0.7 copy-start.8
  54.8 0.8 copy-start.3
  55.6 0.8 copy-start.4

commit v2 on v1

v2 whole, which is shorter than its diff:
```python
import functools
import math

import jax
import jax.numpy as jnp
from jax import lax
from jax.experimental import pallas as pl
from jax.experimental.pallas import tpu as pltpu
from jax.sharding import Mesh
from jax.sharding import PartitionSpec as P

SP = ("sp_0", "sp_1", "sp_2")
SP_TP = ("sp_0", "sp_1", "sp_2", "tp")
MESH = pl.DeviceIdType.MESH

epsilon = 1e-06
max_floor = -1e30
f32 = jnp.float32
bf16 = jnp.bfloat16

NT = (((1,), (1,)), ((), ()))
TN = (((0,), (0,)), ((), ()))
NN = (((1,), (0,)), ((), ()))


def exact(a, b, dims):
    return lax.dot_general(
        a, b, dims, precision=lax.Precision.HIGHEST, preferred_element_type=f32
    )


def mul(a, b, dims=NN):
    return lax.dot_general(a, b, dims, preferred_element_type=f32)


def here():
    return tuple(lax.axis_index(a) for a in SP_TP)


def spots():
    return tuple(lax.axis_size(a) for a in SP_TP)


def flat(at, sizes):
    number = at[0]
    for part, size in zip(at[1:], sizes[1:]):
        number = number * size + part
    return number


def ring(at, size):
    return [at if move == 0 else lax.rem(at + move, size) for move in range(size)]


def hops(moves, sizes):
    return sum(min(move, size - move) for move, size in zip(moves, sizes))


def silu(value):
    return value / (1.0 + jnp.exp(-value))


def layer_kernel(
    heads,
    key_dim,
    value_dim,
    slots,
    group,
    ig_hbm,
    fg_hbm,
    routes_hbm,
    weight_hbm,
    gain_hbm,
    norm_gain_hbm,
    q_hbm,
    k_hbm,
    v_hbm,
    og_hbm,
    res_hbm,
    wout_hbm,
    sg_hbm,
    su_hbm,
    sd_hbm,
    wg_hbm,
    wu_hbm,
    wd_hbm,
    out_ref,
    in_gate,
    forget_gate,
    routes,
    route_weight,
    gain,
    norm_gain,
    q,
    k,
    v,
    og,
    res,
    wout,
    sg,
    su,
    sd,
    wg,
    wu,
    wd,
    out_m,
    in_m,
    back_m,
    state_m,
    out_a,
    in_a,
    back_a,
    state_a,
    local,
    mixed,
    proj_out,
    proj_in,
    proj_own,
    normed,
    rank_ref,
    weight_ref,
    share_high,
    share_low,
    outgoing,
    arrived,
    returned,
    packed,
    answer,
    hidden,
    shared_hidden,
    total_ref,
    gate_sem,
    load_sem,
    state_send,
    state_recv,
    pair_sem,
    send_sem,
    recv_sem,
    send_back,
    recv_back,
):
    sizes = spots()
    places = sizes[0] * sizes[1] * sizes[2]
    two = sizes[3]
    count = places * two
    z, y, x, core = here()
    me = flat((z, y, x), sizes[:3])
    rows = q.shape[0]
    units = 2 * heads
    chunks = places // units
    piece = out_m.shape[1]
    key_scale = 1.0 / math.sqrt(key_dim)
    half, width = res.shape
    tile = 512

    loads = [
        pltpu.make_async_copy(a, b, load_sem.at[n])
        for n, (a, b) in enumerate(
            [
                (k_hbm, k),
                (v_hbm, v),
                (q_hbm, q),
                (og_hbm, og),
                (gain_hbm, gain),
                (norm_gain_hbm, norm_gain),
                (res_hbm, res),
                (wout_hbm, wout),
                (sg_hbm, sg),
                (su_hbm, su),
                (sd_hbm, sd),
                (wg_hbm.at[0], wg),
                (wu_hbm.at[0], wu),
                (wd_hbm.at[0], wd),
                (routes_hbm, routes),
                (weight_hbm, route_weight),
            ]
        )
    ]
    gate_loads = [
        pltpu.make_async_copy(a, b, gate_sem.at[n])
        for n, (a, b) in enumerate([(ig_hbm, in_gate), (fg_hbm, forget_gate)])
    ]
    for load in gate_loads:
        load.start()
    for load in loads[:3]:
        load.start()

    barrier = pltpu.get_barrier_semaphore()
    zs, ys, xs, cores = (ring(at, size) for at, size in zip((z, y, x, core), sizes))
    moves = [
        (dz, dy, dx)
        for dz in range(sizes[0])
        for dy in range(sizes[1])
        for dx in range(sizes[2])
        if (dz, dy, dx) != (0, 0, 0)
    ]
    moves.sort(key=lambda move: (-hops(move, sizes), (move[0] + 2 * move[1] + 3 * move[2]) % 4))
    for dz, dy, dx in moves:
        pl.semaphore_signal(
            barrier, inc=1, device_id=(zs[dz], ys[dy], xs[dx], core), device_id_type=MESH
        )
    partner = (z, y, x, cores[1])
    pl.semaphore_signal(barrier, inc=1, device_id=partner, device_id_type=MESH)

    for load in gate_loads:
        load.wait()
    ig = jnp.concatenate([in_gate[0], in_gate[1]], axis=0)
    fg = jnp.concatenate([forget_gate[0], forget_gate[1]], axis=0)
    decay = jnp.exp(-fg)
    up = 1.0 + decay
    lf = -jnp.where(up == 1.0, decay, jnp.log(up) * (decay / jnp.where(up == 1.0, 1.0, up - 1.0)))
    line = lax.broadcasted_iota(jnp.int32, (rows, rows), 0)
    lane = lax.broadcasted_iota(jnp.int32, (rows, rows), 1)

    def sums_of(value, matrix):
        high = value.astype(bf16).astype(f32)
        middle = (value - high).astype(bf16).astype(f32)
        parts = jnp.concatenate([high, middle, value - high - middle], axis=0).astype(bf16)
        got = mul(parts, matrix.astype(f32).astype(bf16))
        return got[0:units] + (got[units : 2 * units] + got[2 * units :])

    first_row = lax.broadcasted_iota(jnp.int32, (units, rows), 0) < heads
    run_row = jnp.where(first_row, sums_of(lf, line <= lane), sums_of(lf, line >= lane))
    totals = jnp.where(first_row[:, 0:1], run_row[:, rows - 1 : rows], run_row[:, 0:1])
    a_row = totals - run_row + ig
    block_peak = jnp.max(a_row, axis=1, keepdims=True)
    scale_row = jnp.exp(a_row - block_peak) * key_scale
    turned = jnp.concatenate([run_row, scale_row], axis=0).T
    run_col, scale_col = turned[:, 0:units], turned[:, units:]

    loads[0].wait()
    loads[1].wait()
    for load in loads[3:8]:
        load.start()
    for unit in range(units):
        h = unit % heads
        kh = k[:, h * key_dim : (h + 1) * key_dim].astype(f32)
        low = (kh * scale_col[:, unit : unit + 1]).astype(bf16)
        matrix = mul(low, v[:, h * value_dim : (h + 1) * value_dim], TN)
        out_m[unit * chunks : (unit + 1) * chunks] = matrix.astype(bf16).reshape(
            chunks, piece, value_dim
        )
        norm = jnp.sum(low.astype(f32), axis=0, keepdims=True)
        out_a[unit, 0:1, :] = norm
        out_a[unit, 1:2, :] = jnp.broadcast_to(block_peak[unit : unit + 1], (1, key_dim))
        out_a[unit, 2:3, :] = jnp.broadcast_to(totals[unit : unit + 1], (1, key_dim))
        out_a[unit, 3:4, :] = jnp.zeros((1, key_dim), f32)

    pl.semaphore_wait(barrier, places)

    def exchange(phase, src_m, dst_m, src_a, dst_a, a_src, a_dst, with_extra):
        extras = 0
        for dz, dy, dx in moves:
            other = (zs[dz], ys[dy], xs[dx], core)
            spot = flat(other[:3], sizes[:3])
            pairs = [(src_m.at[spot], dst_m.at[me])]
            if with_extra(dz, dy, dx):
                pairs.append((src_a.at[a_src(spot)], dst_a.at[a_dst(me)]))
                extras += 1
            for n, (src, dst) in enumerate(pairs):
                pltpu.make_async_remote_copy(
                    src_ref=src,
                    dst_ref=dst,
                    send_sem=state_send.at[phase, n],
                    recv_sem=state_recv.at[phase, n],
                    device_id=other,
                    device_id_type=MESH,
                ).start()
        dst_m[me] = src_m[me]
        dst_a[a_dst(me)] = src_a[a_src(me)]

        def all_of(sems):
            for n, (dst, number) in enumerate([(dst_m, places - 1), (dst_a, extras)]):
                part = dst.at[pl.ds(0, number)]
                pltpu.make_async_copy(part, part, sems.at[phase, n]).wait()

        return all_of

    first = exchange(
        0,
        out_m,
        in_m,
        out_a,
        in_a,
        lambda spot: spot // chunks,
        lambda spot: spot,
        lambda dz, dy, dx: True,
    )

    for load in loads[8:]:
        load.start()

    loads[2].wait()
    peaks, sums = [], []
    for h in range(heads):
        qh = q[:, h * key_dim : (h + 1) * key_dim]
        kh = k[:, h * key_dim : (h + 1) * key_dim]
        vh = v[:, h * value_dim : (h + 1) * value_dim]
        scores = mul(qh, kh, NT) * key_scale
        for way in range(2):
            unit = way * heads + h
            seen = (line >= lane) if way == 0 else (line <= lane)
            pair = run_col[:, unit : unit + 1] + (ig[unit : unit + 1] - run_row[unit : unit + 1])
            pair = jnp.where(seen, pair, max_floor)
            top = jnp.max(pair, axis=1, keepdims=True)
            weight = jnp.where(seen, jnp.exp(pair - top), 0.0) * scores
            local[unit] = mul(weight.astype(bf16), vh)
            peaks.append(top)
            sums.append(jnp.sum(weight, axis=1, keepdims=True))

    first(state_recv)
    backward = me // (chunks * heads)

    def advance(s, carry):
        m, n, top = carry
        at = s + backward * (places - 1 - 2 * s)
        back_m[at] = m.astype(bf16)
        back_a[at, 0:1, :] = n
        back_a[at, 1:2, :] = top
        block_top = in_a[at, 1:2, :]
        moved = in_a[at, 2:3, :] + top
        new = jnp.maximum(moved, block_top)
        keep = jnp.exp(moved - new)
        add = jnp.exp(block_top - new)
        wide_keep = jnp.concatenate([keep] * (value_dim // key_dim), axis=1)
        wide_add = jnp.concatenate([add] * (value_dim // key_dim), axis=1)
        m = wide_keep * m + wide_add * in_m[at].astype(f32)
        n = keep * n + add * in_a[at, 0:1, :]
        return m, n, new

    lax.fori_loop(
        0,
        places,
        advance,
        (
            jnp.zeros((piece, value_dim), f32),
            jnp.zeros((1, key_dim), f32),
            jnp.full((1, key_dim), max_floor, f32),
        ),
        unroll=4,
    )
    second = exchange(
        1,
        back_m,
        state_m,
        back_a,
        state_a,
        lambda spot: spot,
        lambda spot: spot // chunks,
        lambda dz, dy, dx: (dy * sizes[2] + dx) % chunks == 0,
    )

    for load in loads[14:]:
        load.wait()

    expert = lax.broadcasted_iota(jnp.int32, (count, half), 0)
    named = jnp.zeros((count, half), f32)
    share = jnp.zeros((count, half), f32)
    for n in range(routes.shape[0]):
        hit = expert == routes[n : n + 1, :]
        named = named + hit.astype(f32)
        share = share + jnp.where(hit, route_weight[n : n + 1, :], 0.0)
    earlier = (
        lax.broadcasted_iota(jnp.int32, (half, half), 0)
        < lax.broadcasted_iota(jnp.int32, (half, half), 1)
    ).astype(bf16)
    rank_ref[...] = jnp.where(named > 0.0, mul(named.astype(bf16), earlier), -1.0)
    weight_ref[...] = share
    block = group
    slot = lax.broadcasted_iota(jnp.int32, (block, slots, half), 1).astype(f32)

    def peers(b, sign):
        outer, inner = b // two, lax.rem(b, two) * two

        if sign < 0:
            zb = [lax.rem(z + 2 * sizes[0] - (outer + m), sizes[0]) for m in range(sizes[0])]
            yb = [lax.rem(y + 2 * sizes[1] - (inner + m), sizes[1]) for m in range(sizes[1])]
        else:
            zb = [lax.rem(z + outer + m, sizes[0]) for m in range(sizes[0])]
            yb = [lax.rem(y + inner + m, sizes[1]) for m in range(sizes[1])]
        out = []
        for n in range(block):
            dc, dx, rest = n % two, (n // two) % sizes[2], n // (two * sizes[2])
            dz = (2 * dx + dc) % sizes[0]
            dy = (rest + dx + 2 * dc) % sizes[1]
            out.append((zb[dz], yb[dy], xs[dx if sign > 0 else -dx], cores[dc]))
        return out

    def lines_of(ref, b):
        at = [flat(peer, sizes) for peer in peers(b, 1)]
        return jnp.concatenate([ref[pl.ds(one, 1), :] for one in at], axis=0)

    def picks(b):
        return (lines_of(rank_ref, b)[:, None, :] == slot).astype(f32)

    def sharing(b, carry):
        weights = picks(b) * lines_of(weight_ref, b)[:, None, :]
        turned = weights.reshape(block * slots, half).T
        high = turned.astype(bf16)
        share_high[b] = high
        share_low[b] = (turned - high.astype(f32)).astype(bf16)
        return carry

    lax.fori_loop(0, count // block, sharing, 0)

    loads[3].wait()
    loads[4].wait()
    second(state_recv)

    for h in range(heads):
        qh = q[:, h * key_dim : (h + 1) * key_dim]
        qw = qh.astype(f32)
        total = None
        for way in range(2):
            unit = way * heads + h
            state = state_m[unit * chunks : (unit + 1) * chunks].reshape(key_dim, value_dim)
            norm = state_a[unit, 0:1, :]
            top = state_a[unit, 1:2, :]
            crossing = run_col[:, unit : unit + 1] + top[:, 0:1]
            row_max = jnp.maximum(crossing, peaks[h * 2 + way])
            carry = jnp.exp(crossing - row_max)
            inner = jnp.exp(peaks[h * 2 + way] - row_max)
            read_norm = jnp.sum(qw * norm, axis=1, keepdims=True)
            divisor = carry * read_norm + inner * sums[h * 2 + way]
            divisor = jnp.maximum(jnp.abs(divisor), jnp.exp(-row_max))
            part = (carry * mul(qh, state) + inner * local[unit]) / divisor
            total = part if total is None else total + part
        normal = total * lax.rsqrt(jnp.mean(total * total, axis=1, keepdims=True) + epsilon)
        span = slice(h * value_dim, (h + 1) * value_dim)
        gate = 1.0 / (1.0 + jnp.exp(-og[:, span].astype(f32)))
        mixed[:, span] = (normal * gain[:, span] * gate).astype(bf16)

    for load in loads[5:8]:
        load.wait()
    tiles = [slice(n * tile, (n + 1) * tile) for n in range(width // tile)]
    trades = []
    for n, cols in enumerate(tiles):
        both = mul(mixed[...], wout[:, cols])
        proj_out[n] = jnp.where(core == 0, both[half:], both[:half]).astype(bf16)
        trades.append(
            pltpu.make_async_remote_copy(
                src_ref=proj_out.at[n],
                dst_ref=proj_in.at[n],
                send_sem=pair_sem.at[0, n],
                recv_sem=pair_sem.at[1, n],
                device_id=partner,
                device_id_type=MESH,
            )
        )
        trades[-1].start()
        own = jnp.where(core == 0, both[:half], both[half:])
        proj_own[:, cols] = res[:, cols].astype(f32) + own
    squares = jnp.zeros((half, 1), f32)
    for n, cols in enumerate(tiles):
        trades[n].wait()
        wide = (proj_own[:, cols] + proj_in[n].astype(f32)).astype(bf16).astype(f32)
        total_ref[:, cols] = wide
        squares = squares + jnp.sum(wide * wide, axis=1, keepdims=True)
    level = lax.rsqrt(squares * (1.0 / width) + epsilon)
    for cols in tiles:
        normed[:, cols] = (total_ref[:, cols] * level * norm_gain[:, cols]).astype(bf16)

    def dispatch(b, n, other):
        i = b * block + n
        return pltpu.make_async_remote_copy(
            src_ref=outgoing.at[i],
            dst_ref=arrived.at[i],
            send_sem=send_sem,
            recv_sem=recv_sem.at[b],
            device_id=other,
            device_id_type=MESH,
        )

    def give_back(b, n, other):
        i = b * block + n
        return pltpu.make_async_remote_copy(
            src_ref=answer.at[i],
            dst_ref=returned.at[i],
            send_sem=send_back,
            recv_sem=recv_back.at[b],
            device_id=other,
            device_id_type=MESH,
        )

    def start_all(b, copy, sign):
        others = peers(b, sign)

        @pl.when(b > 0)
        def _():
            copy(b, 0, others[0]).start()

        for n in range(1, block):
            copy(b, n, others[n]).start()

    def bytes_of(rows_ref, sem):
        pltpu.make_async_copy(rows_ref, rows_ref, sem).wait()

    def landed(b, sems, rows_ref):
        @pl.when(b == 0)
        def _():
            bytes_of(rows_ref.at[pl.ds(1, block - 1)], sems.at[0])

        @pl.when(b > 0)
        def _():
            bytes_of(rows_ref.at[pl.ds(b * block, block)], sems.at[b])

    def fill(b, carry):
        lines = pl.ds(pl.multiple_of(b * block, block), block)
        pick = picks(b).reshape(block * slots, half).astype(bf16)
        moved = mul(pick, normed[...])
        outgoing[lines] = moved.reshape(block, slots, width).astype(bf16)
        start_all(b, dispatch, 1)
        return carry

    lax.fori_loop(0, count // block, fill, 0)
    arrived[0] = outgoing[0]

    for load in loads[8:11]:
        load.wait()
    shared_hidden[...] = (silu(mul(normed[...], sg[...])) * mul(normed[...], su[...])).astype(bf16)

    def shared_part(n, carry):
        cols = pl.ds(pl.multiple_of(n * tile, tile), tile)
        total_ref[:, cols] = total_ref[:, cols] + mul(shared_hidden[...], sd[:, cols])
        return carry

    lax.fori_loop(0, width // tile, shared_part, 0)
    for load in loads[11:14]:
        load.wait()

    def work(g, carry):
        landed(g, recv_sem, arrived)
        sources = pl.ds(pl.multiple_of(g * group, group), group)
        packed[...] = arrived[sources].astype(f32).reshape(group * slots, width).astype(bf16)
        hidden[...] = (silu(mul(packed[...], wg[...])) * mul(packed[...], wu[...])).astype(bf16)

        def down(n, inner):
            cols = pl.ds(pl.multiple_of(n * tile, tile), tile)
            answer[sources, :, cols] = (
                mul(hidden[...], wd[:, cols]).reshape(group, slots, tile).astype(bf16)
            )
            return inner

        lax.fori_loop(0, width // tile, down, 0)
        start_all(g, give_back, -1)
        return carry

    lax.fori_loop(0, count // group, work, 0)
    returned[0] = answer[0]

    def collect(b, carry):
        landed(b, recv_back, returned)
        lines = pl.ds(pl.multiple_of(b * block, block), block)

        def part(n, inner):
            cols = pl.ds(pl.multiple_of(n * tile, tile), tile)
            landed = returned[lines, :, cols].astype(f32).reshape(block * slots, tile).astype(bf16)
            total_ref[:, cols] = total_ref[:, cols] + (
                mul(share_high[b], landed) + mul(share_low[b], landed)
            )
            return inner

        lax.fori_loop(0, width // tile, part, 0)
        return carry

    lax.fori_loop(0, count // block, collect, 0)
    out_ref[...] = total_ref[...].astype(bf16)

    bytes_of(outgoing.at[pl.ds(1, count - 1)], send_sem)
    bytes_of(answer.at[pl.ds(1, count - 1)], send_back)
    first(state_send)
    second(state_send)


def local(
    residual,
    queries,
    keys,
    values,
    out_gate,
    in_gate,
    forget_gate,
    head_gain,
    w_out,
    norm_gain,
    shared_gate,
    shared_up,
    shared_down,
    w_gate,
    w_up,
    w_down,
    routes,
    route_weight,
):
    rows = queries.shape[0]
    heads = in_gate.shape[2]
    key_dim, value_dim = queries.shape[1] // heads, values.shape[1] // heads
    places = math.prod(lax.axis_size(a) for a in SP)
    count = places * lax.axis_size("tp")
    units = 2 * heads
    piece = key_dim * units // places
    half, width = residual.shape
    slots = half * routes.shape[1] * lax.axis_size("tp") // count
    group = 16
    block = 16
    hidden = w_gate.shape[2]
    vmem = pl.BlockSpec(memory_space=pltpu.VMEM)
    hbm = pl.BlockSpec(memory_space=pltpu.HBM)
    matrices = pltpu.VMEM((places, piece, value_dim), bf16)
    extras = pltpu.VMEM((places, 4, key_dim), f32)
    slot_rows = pltpu.VMEM((count, slots, width), bf16)
    return pl.pallas_call(
        functools.partial(layer_kernel, heads, key_dim, value_dim, slots, group),
        out_shape=pltpu.VMEM((half, width), bf16),
        in_specs=[hbm] * 18,
        out_specs=vmem,
        scratch_shapes=[
            pltpu.VMEM((2, heads, rows), f32),
            pltpu.VMEM((2, heads, rows), f32),
            pltpu.VMEM((routes.shape[1], half), jnp.int32),
            pltpu.VMEM((routes.shape[1], half), f32),
            pltpu.VMEM((1, head_gain.shape[0]), f32),
            pltpu.VMEM((1, width), f32),
            pltpu.VMEM(queries.shape, bf16),
            pltpu.VMEM(keys.shape, bf16),
            pltpu.VMEM(values.shape, bf16),
            pltpu.VMEM(out_gate.shape, bf16),
            pltpu.VMEM(residual.shape, bf16),
            pltpu.VMEM(w_out.shape, bf16),
            pltpu.VMEM(shared_gate.shape, bf16),
            pltpu.VMEM(shared_up.shape, bf16),
            pltpu.VMEM(shared_down.shape, bf16),
            pltpu.VMEM(w_gate.shape[1:], bf16),
            pltpu.VMEM(w_up.shape[1:], bf16),
            pltpu.VMEM(w_down.shape[1:], bf16),
            matrices,
            matrices,
            matrices,
            matrices,
            pltpu.VMEM((units, 4, key_dim), f32),
            extras,
            extras,
            pltpu.VMEM((units, 4, key_dim), f32),
            pltpu.VMEM((units, rows, value_dim), f32),
            pltpu.VMEM(values.shape, bf16),
            pltpu.VMEM((width // 512, half, 512), bf16),
            pltpu.VMEM((width // 512, half, 512), bf16),
            pltpu.VMEM((half, width), f32),
            pltpu.VMEM((half, width), bf16),
            pltpu.VMEM((count, half), f32),
            pltpu.VMEM((count, half), f32),
            pltpu.VMEM((count // block, half, block * slots), bf16),
            pltpu.VMEM((count // block, half, block * slots), bf16),
            slot_rows,
            slot_rows,
            slot_rows,
            pltpu.VMEM((group * slots, width), bf16),
            slot_rows,
            pltpu.VMEM((group * slots, hidden), bf16),
            pltpu.VMEM((half, shared_gate.shape[1]), bf16),
            pltpu.VMEM((half, width), f32),
            pltpu.SemaphoreType.DMA((2,)),
            pltpu.SemaphoreType.DMA((16,)),
            pltpu.SemaphoreType.DMA((2, 2)),
            pltpu.SemaphoreType.DMA((2, 2)),
            pltpu.SemaphoreType.DMA((2, width // 512)),
            pltpu.SemaphoreType.DMA,
            pltpu.SemaphoreType.DMA((count // block,)),
            pltpu.SemaphoreType.DMA,
            pltpu.SemaphoreType.DMA((count // block,)),
        ],
        compiler_params=pltpu.CompilerParams(
            collective_id=0, has_side_effects=True, vmem_limit_bytes=56 * 1024 * 1024
        ),
        name="layer",
    )(
        in_gate.transpose(0, 2, 1),
        forget_gate.transpose(0, 2, 1),
        routes.T,
        route_weight.T,
        head_gain.reshape(1, -1),
        norm_gain.reshape(1, -1),
        queries,
        keys,
        values,
        out_gate,
        residual,
        w_out,
        shared_gate,
        shared_up,
        shared_down,
        w_gate,
        w_up,
        w_down,
    )


def solution(mesh):
    finer = Mesh(mesh.devices.reshape(4, 4, 4, mesh.shape["tp"]), SP_TP)
    return jax.shard_map(
        local,
        mesh=finer,
        in_specs=(
            P(SP_TP, None),
            P(SP, "tp"),
            P(SP, "tp"),
            P(SP, "tp"),
            P(SP, "tp"),
            P(None, SP, "tp"),
            P(None, SP, "tp"),
            P("tp"),
            P("tp", None),
            P(),
            P(),
            P(),
            P(),
            P(SP_TP, None, None),
            P(SP_TP, None, None),
            P(SP_TP, None, None),
            P(SP_TP, None),
            P(SP_TP, None),
        ),
        out_specs=P(SP_TP, None),
        check_vma=False,
    )
```

time: 169 us -> 130 us (0.77)
  Pallas kernels: 155 us -> 129 us
  local copies, waits for them, and re-layouts: 12.7 us -> 0.8 us
    pallas_call x2 -> x1, Pallas kernels: 155 us -> 129 us  [local(): pl.pallas_call(functools.partial(layer_kernel, heads, key_dim, value_dim,...]
    unnamed x21 -> x1, local copies, waits for them, and re-layouts: 12.7 us -> 0.8 us
where the time goes in v2:
time: 130 us
  Pallas kernels  129 us (99%)
    pallas_call x1, Pallas kernels, local(): pl.pallas_call(functools.partial(layer_kernel, heads, key_dim, value_dim,...  129 us

profile of v2, /device:TPU:1, one launch (start us, length us, event | category | flops | bytes accessed | tf_op | source)
XLA Modules:
  0.0 130.2 jit_solution(4383704816397464252)
XLA Ops:
  0.0 129.4 %layer.1 = bf16[128,2048]{1,0:T(8,128)(2,1)S(1)} custom-call(f32[2,4,256]{2,1,0:T(4,128)} %bitcast.6, f32[2,4,256]{2,1,0:T(4,128)} %bitcast.7, s32[4,128]{1,0:T(4,128)} %bitcast.10, f32[4,128]{1,0:T(4,128)} %bitcast.11, f32[1,1024]{1,0:T(1,128)} %bitcast.9, f32[1,2048]{1,0:T(1,128)} %bitcast.8, bf16[256,512]{1,0:T(8,128)(2,1)} %q_hbm.1, ...), custom_call_target="tpu_custom_call" | custom-call | tf_op jit(solution)/shard_map/layer/pallas_call | solution.py:612
  129.4 0.8 copy.20
